TPU v7x, 32 devices: a whole 2x2x4 slice. The times are simulated.
32 devices in a mesh: ep: 8 (over z, core), tp: 4 (over y, x).
Axes of the slice: x: 2, y: 2, z: 4, core: 2. Of those that a mesh axis runs over, the one named last changes fastest.
Arguments:
- query_rows: bfloat16 [3072, 2048], P('ep', 'tp'), may hold values from -6 to 6
- key_rows: bfloat16 [3072, 2048], P('ep', 'tp'), may hold values from -6 to 6
- value_rows: bfloat16 [3072, 2048], P('ep', 'tp'), may hold values from -6 to 6
- second_scale: float32 [16], P('tp'), may hold values from 0.3 to 0.8
- head_gain: float32 [128], replicated, may hold values from 0.1 to 1.9
- out_weight: bfloat16 [2048, 4096], P(None, 'tp'), may hold values from -0.125 to 0.125
- routed_rows: bfloat16 [1024, 4096], P('ep', 'tp'), may hold values from -6 to 6
- norm_gain: float32 [4096], replicated, may hold values from 0.1 to 1.9
- route_ids: int32 [1024, 2], P('ep'), may hold values from 0 to 7, all different within a row; in each aligned block of 128 rows (0 to 127, 128 to 255, ...) at most 64 rows name the same one
- route_weight: float32 [1024, 2], P('ep'), may hold values from 0.1 to 0.9
- expert_gate: bfloat16 [8, 4096, 2048], P('ep', None, 'tp'), may hold values from -0.09375 to 0.09375
- expert_up: bfloat16 [8, 4096, 2048], P('ep', None, 'tp'), may hold values from -0.09375 to 0.09375
- expert_down: bfloat16 [8, 2048, 4096], P('ep', None, 'tp'), may hold values from -0.125 to 0.125
Outputs:
- mixer_out: bfloat16 [3072, 4096], P('ep', 'tp')
- expert_mix: bfloat16 [1024, 4096], P('ep', 'tp')
Inputs may be any that keep to these rules, and one draw needn't show every extreme that they name: `route_ids`: among the 128 tokens of one index of ep, no expert is named by more than 64 of them, a bound that some block reaches.
All inputs are finite; a program needn't handle non-finite values.
Results may differ from a plain program's by a relative error of at most 0.0085.
Values may be sent and summed in bfloat16 or wider, within the bound.
A program may use at most 128 MiB of HBM per device.

v0:
```python
import jax
import jax.numpy as jnp
from jax import lax
from jax.sharding import PartitionSpec as P

eps = 1e-06
head_factor = 0.8
neg_big = -1e30
key_block_rows = 1024


def rms_rows(rows_in, gain):
    floats = rows_in.astype(jnp.float32)
    factor = lax.rsqrt(jnp.mean(floats * floats, axis=-1, keepdims=True) + eps)
    return (floats * factor * gain).astype(jnp.bfloat16)


def per_device(
    query_rows,
    key_rows,
    value_rows,
    second_scale,
    head_gain,
    out_weight,
    routed_rows,
    norm_gain,
    route_ids,
    route_weight,
    expert_gate,
    expert_up,
    expert_down,
):
    count_a = query_rows.shape[0]
    per_head = second_scale.shape[0]
    head_dim = query_rows.shape[1] // (2 * per_head)
    value_dim = head_gain.shape[0]
    query_four = query_rows.reshape(count_a, per_head, 2, head_dim)
    query_pos = lax.axis_index("ep") * count_a + jnp.arange(count_a, dtype=jnp.int32)

    def key_block(carry_state, key_part, value_part, block_start):
        key_count = key_part.shape[0]
        key_four = key_part.reshape(key_count, per_head, 2, head_dim)
        value_three = value_part.reshape(key_count, per_head, value_dim)
        scores = jnp.einsum(
            "ihcd,jhcd->ihcj", query_four, key_four, preferred_element_type=jnp.float32
        ) * head_dim ** (-0.5)
        allowed = (
            query_pos[:, None] >= block_start + jnp.arange(key_count, dtype=jnp.int32)[None, :]
        )[:, None, None, :]
        scores = jnp.where(allowed, scores, neg_big)
        old_max, old_sum, old_acc = carry_state
        new_max = jnp.maximum(old_max, jnp.max(scores, axis=-1))
        weights = jnp.where(allowed, jnp.exp(scores - new_max[..., None]), 0.0)
        shrink = jnp.exp(old_max - new_max)
        new_sum = old_sum * shrink + jnp.sum(weights, axis=-1)
        update = jnp.einsum(
            "ihcj,jhe->ihce",
            weights.astype(jnp.bfloat16),
            value_three,
            preferred_element_type=jnp.float32,
        )
        return (new_max, new_sum, old_acc * shrink[..., None] + update)

    start_state = (
        jnp.full((count_a, per_head, 2), neg_big, jnp.float32),
        jnp.zeros((count_a, per_head, 2), jnp.float32),
        jnp.zeros((count_a, per_head, 2, value_dim), jnp.float32),
    )
    key_part = lax.all_gather(key_rows, "ep", axis=0, tiled=True)
    value_part = lax.all_gather(value_rows, "ep", axis=0, tiled=True)
    key_count = key_part.shape[0]

    def step_block(block_num, inner_state):
        offset_rows = block_num * key_block_rows
        key_slice = lax.dynamic_slice_in_dim(key_part, offset_rows, key_block_rows, 0)
        value_slice = lax.dynamic_slice_in_dim(value_part, offset_rows, key_block_rows, 0)
        return key_block(inner_state, key_slice, value_slice, offset_rows)

    run_max, run_sum, run_acc = lax.fori_loop(
        0, key_count // key_block_rows, step_block, start_state
    )
    maps_both = run_acc / run_sum[..., None]
    mixed_maps = maps_both[:, :, 0] - second_scale[None, :, None] * maps_both[:, :, 1]
    mean_sq = jnp.mean(mixed_maps * mixed_maps, axis=-1, keepdims=True)
    head_out = (
        (mixed_maps * lax.rsqrt(mean_sq + eps) * head_gain * head_factor)
        .astype(jnp.bfloat16)
        .reshape(count_a, per_head * value_dim)
    )
    count_b = routed_rows.shape[0]
    route_count = route_ids.shape[1]
    experts_here = expert_gate.shape[0]
    ep_devices = lax.axis_size("ep")
    expert_total = experts_here * ep_devices
    capacity = 2 * count_b * route_count // expert_total
    flat_expert = route_ids.reshape(-1)
    chosen = (flat_expert[:, None] == jnp.arange(expert_total, dtype=jnp.int32)[None, :]).astype(
        jnp.int32
    )
    ranks = jnp.sum((jnp.cumsum(chosen, axis=0) - 1) * chosen, axis=1)
    slot_of = flat_expert * capacity + ranks
    token_of = jnp.arange(count_b * route_count, dtype=jnp.int32) // route_count
    slot_token = jnp.full((expert_total * capacity,), count_b, jnp.int32).at[slot_of].set(token_of)
    padded = jnp.concatenate(
        [routed_rows, jnp.zeros((1, routed_rows.shape[1]), jnp.bfloat16)], axis=0
    )
    outgoing = padded[slot_token].reshape(ep_devices, experts_here, capacity, routed_rows.shape[1])
    column_parts = lax.all_to_all(outgoing, "ep", split_axis=0, concat_axis=0, tiled=True)
    arrived = rms_rows(lax.all_gather(column_parts, "tp", axis=3, tiled=True), norm_gain)
    gate_val = jnp.einsum(
        "sxcd,xdf->sxcf", arrived, expert_gate, preferred_element_type=jnp.float32
    )
    up_val = jnp.einsum("sxcd,xdf->sxcf", arrived, expert_up, preferred_element_type=jnp.float32)
    hidden = (jax.nn.silu(gate_val) * up_val).astype(jnp.bfloat16)
    weight_rows = out_weight
    attn_total = jnp.dot(
        lax.all_gather(
            head_out.reshape(1, 1, count_a, head_out.shape[1]), "tp", axis=3, tiled=True
        )[0, 0],
        weight_rows,
        preferred_element_type=jnp.float32,
    )
    weight_rows = expert_down
    moe_total = jnp.einsum(
        "sxcf,xfd->sxcd",
        lax.all_gather(hidden, "tp", axis=3, tiled=True),
        weight_rows,
        preferred_element_type=jnp.float32,
    )
    mixer_out = attn_total.astype(jnp.bfloat16)
    returned = lax.all_to_all(
        moe_total.astype(jnp.bfloat16), "ep", split_axis=0, concat_axis=0, tiled=True
    )
    flat_back = returned.reshape(expert_total * capacity, returned.shape[3])
    picked = flat_back[slot_of].astype(jnp.float32).reshape(count_b, route_count, returned.shape[3])
    expert_mix = jnp.sum(picked * route_weight[:, :, None], axis=1).astype(jnp.bfloat16)
    return (mixer_out, expert_mix)


def solution(mesh):
    placed = (
        P("ep", "tp"),
        P("ep", "tp"),
        P("ep", "tp"),
        P("tp"),
        P(),
        P(None, "tp"),
        P("ep", "tp"),
        P(),
        P("ep", None),
        P("ep", None),
        P("ep", None, "tp"),
        P("ep", None, "tp"),
        P("ep", None, "tp"),
    )
    return jax.shard_map(
        per_device,
        mesh=mesh,
        in_specs=placed,
        out_specs=(P("ep", "tp"), P("ep", "tp")),
        check_vma=False,
    )
```

profile of v0, /device:TPU:24, one launch (start us, length us, event | category | flops | bytes accessed | tf_op | source)
XLA Modules:
  0.0 285.7 jit_solution(6418652989304294273)
XLA Ops:
  7.2 0.0 all-gather.12.cloned.1.call-start
  7.2 0.7 broadcast_multiply_fusion
  7.9 0.8 copy.36
  8.7 0.1 eq.29
  8.8 0.1 eq.25
  9.0 0.1 copy.35
  9.1 0.1 mul.194
  9.2 0.6 reduce-window.6
  9.8 0.2 slice_reduce_fusion
  10.1 0.1 fusion.65
  10.2 1.4 scatter_custom_fusion
  11.6 1.0 concatenate.3
  12.6 2.1 gather_fusion
  14.7 29.2 %all_to_all.10 = bf16[8,1,64,1024]{3,2,1,0:T(8,128)(2,1)} all-to-all(bf16[8,1,64,1024]{3,2,1,0:T(8,128)(2,1)S(1)} %bitcast.152), channel_id=1, replica_groups=mesh['ep'=8,'tp'=4] {'ep'}, dimensions={0} | all-to-all | bytes 2097152 | tf_op jit(solution)/shard_map/all_to_all | solution.py:108
  43.9 0.0 all-gather.12.cloned.1.call-update
  43.9 0.0 all-gather.6.cloned.1.call-start
  44.0 0.9 copy.31
  44.9 0.0 all-gather.8.cloned.1.call-start
  45.0 0.9 copy.33
  45.9 0.0 all-gather.8.cloned.1.call-update
  45.9 0.0 all-gather.14.cloned.1.call-start
  46.0 1.2 copy.32
  47.2 0.1 broadcast_bitcast_fusion
  47.3 50.3 %all-gather.12.cloned.1.call-done = bf16[8,1,64,4096]{3,2,1,0:T(8,128)(2,1)} async-done(((bf16[8,1,64,1024]{3,2,1,0:T(8,128)(2,1)}), bf16[8,1,64,4096]{3,2,1,0:T(8,128)(2,1)}) %all-gather.12.cloned.1.call-update) | async-done | bytes 4194320 | tf_op jit(solution)/shard_map/all_gather | solution.py:109
  97.6 3.2 %fusion.15 = f32[8,64]{1,0:T(8,128)S(1)} fusion(bf16[8,1,64,4096]{3,2,1,0:T(8,128)(2,1)} %all-gather.12.cloned.1.call-done), kind=kLoop, calls=%fused_computation.28 | loop fusion | flops 6290944 | bytes 4196352 | tf_op jit(solution)/shard_map/reduce_sum | solution.py:14
  100.8 0.2 copy-done.1
  101.1 4.7 %fusion.43 = f32[8,1,64,512]{3,2,0,1:T(8,128)S(1)} fusion(bf16[1,4096,512]{2,1,0:T(8,128)(2,1)} %param.25, bf16[8,1,64,4096]{3,2,1,0:T(8,128)(2,1)S(1)} %copy-done.1, f32[4096]{0:T(1024)S(1)} %copy-done.8, f32[8,64]{1,0:T(8,128)S(1)} %add_rsqrt_fusion.1), kind=kOutput, calls=%fused_computation.44 | convolution fusion | flops 2155872256 | bytes 9455616 | tf_op jit(solution)/shard_map/sxcd,xdf->sxcf/dot_general | solution.py:110
  105.8 3.3 %fusion.58 = bf16[8,1,64,512]{3,2,0,1:T(8,128)(2,1)} fusion(bf16[1,4096,512]{2,1,0:T(8,128)(2,1)S(1)} %copy-done.7, bf16[8,1,64,4096]{3,2,1,0:T(8,128)(2,1)S(1)} %copy-done.1, f32[4096]{0:T(1024)S(1)} %copy-done.8, f32[8,64]{1,0:T(8,128)S(1)} %add_rsqrt_fusion.1, f32[8,1,64,512]{3,2,0,1:T(8,128)S(1)} %fusion.43), kind=kOutput, calls=%fused_computation.47 | convolution fusion | flops 2157445120 | bytes 9979904 | tf_op jit(solution)/shard_map/sxcd,xdf->sxcf/dot_general | solution.py:113
  109.1 0.2 all-gather.10.cloned.1.call-start
  109.3 26.1 %all-gather.6.cloned.1.call-done = bf16[3072,512]{0,1:T(8,128)(2,1)} async-done(((bf16[384,512]{0,1:T(8,128)(2,1)}), bf16[3072,512]{0,1:T(8,128)(2,1)}) %all-gather.6.cloned.1.call-update) | async-done | bytes 3145744 | tf_op jit(solution)/shard_map/all_gather | solution.py:69
  135.4 38.8 %all-gather.8.cloned.1.call-done = bf16[3072,512]{0,1:T(8,128)(2,1)} async-done(((bf16[384,512]{0,1:T(8,128)(2,1)}), bf16[3072,512]{0,1:T(8,128)(2,1)}) %all-gather.8.cloned.1.call-update) | async-done | bytes 3145744 | tf_op jit(solution)/shard_map/all_gather | solution.py:70
  174.1 62.3 %while.18 = (s32[]{:T(128)}, f32[384,4,2]{0,2,1:T(2,128)S(1)}, f32[384,4,2]{0,2,1:T(2,128)S(1)}, f32[384,4,2,128]{0,3,2,1:T(8,128)S(1)}, bf16[3072,512]{0,1:T(8,...) while((s32[]{:T(128)}, f32[384,4,2]{0,2,1:T(2,128)S(1)}, ...), condition=%wide.region_3.4_spmd.clone, body=%wide.region_0.3_spmd.clone.sunk | while | flops 1250443648 | bytes 99691744 | solution.py:79
  174.1 0.3 broadcast_compare_fusion.2
  174.4 1.7 constant_dynamic-slice_fusion.3
  176.2 6.7 %fusion.86 = (f32[384,4,2]{0,2,1:T(2,128)S(1)}, f32[4,2,1024,384]{3,2,1,0:T(8,128)}) fusion(pred[384,1024]{0,1:T(8,128)(4,1)S(1)} %broadcast_compare_fusion.2, bf16[1024,4,2,64]{0,3,2,1:T(8,128)(2,1)S(1)} %bitcast.148, bf16[384,4,2,64]{0,3,2,1:T(8,128)(2,1)S(1)} %get-tuple-element.290), kind=kOutput, calls=%fused_computation.6.clone.1 | convolution fusion | flops 412087296 | bytes 14430208 | tf_op jit(solution)/shard_map/while/body/eval_jaxpr/ihcd,jhcd->ihcj/dot_general | solution.py:44
  182.9 7.1 %fusion.88 = f32[384,4,2]{0,2,1:T(2,128)S(1)} fusion(f32[4,2,1024,384]{3,2,1,0:T(8,128)} %get-tuple-element.257, f32[384,4,2]{0,2,1:T(2,128)S(1)} %fusion.87, pred[384,1024]{0,1:T(8,128)(4,1)S(1)} %broadcast_compare_fusion.2), kind=kLoop, calls=%fused_computation.8.clone.1 | loop fusion | flops 15725568 | bytes 13000704 | tf_op jit(solution)/shard_map/while/body/eval_jaxpr/reduce_sum | solution.py:55
  190.0 1.7 copy-done
  191.7 3.6 %bitcast_add_fusion.2 = f32[384,4,2,128]{0,3,2,1:T(8,128)S(1)} fusion(f32[384,4,2,128]{0,3,2,1:T(8,128)S(1)} %get-tuple-element.276, bf16[1024,4,128,1]{0,2,3,1:T(8,128)(2,1)S(1)} %bitcast.149, f32[4,2,1024,384]{3,2,1,0:T(8,128)S(1)} %copy-done, f32[384,4,2]{0,2,1:T(2,128)S(1)} %fusion.87, pred[384,1024]{0,1:T(8,128)(4,1)S(1)} %broadcast_compare_fusion.2, ...), kind=kOutput, calls=%fused_computation.11.clone.1 | convolution fusion | flops 822214656 | bytes 17195008 | tf_op jit(solution)/shard_map/while/body/eval_jaxpr/ihcj,jhe->ihce/dot_general | solution.py:56
  195.3 0.3 broadcast_compare_fusion.2
  195.6 1.7 constant_dynamic-slice_fusion.3
  197.3 6.7 %fusion.86 = (f32[384,4,2]{0,2,1:T(2,128)S(1)}, f32[4,2,1024,384]{3,2,1,0:T(8,128)}) fusion(pred[384,1024]{0,1:T(8,128)(4,1)S(1)} %broadcast_compare_fusion.2, bf16[1024,4,2,64]{0,3,2,1:T(8,128)(2,1)S(1)} %bitcast.148, bf16[384,4,2,64]{0,3,2,1:T(8,128)(2,1)S(1)} %get-tuple-element.290), kind=kOutput, calls=%fused_computation.6.clone.1 | convolution fusion | flops 412087296 | bytes 14430208 | tf_op jit(solution)/shard_map/while/body/eval_jaxpr/ihcd,jhcd->ihcj/dot_general | solution.py:44
  204.0 6.8 %fusion.88 = f32[384,4,2]{0,2,1:T(2,128)S(1)} fusion(f32[4,2,1024,384]{3,2,1,0:T(8,128)} %get-tuple-element.257, f32[384,4,2]{0,2,1:T(2,128)S(1)} %fusion.87, pred[384,1024]{0,1:T(8,128)(4,1)S(1)} %broadcast_compare_fusion.2), kind=kLoop, calls=%fused_computation.8.clone.1 | loop fusion | flops 15725568 | bytes 13000704 | tf_op jit(solution)/shard_map/while/body/eval_jaxpr/reduce_sum | solution.py:55
  210.8 1.4 copy-done
  212.3 3.6 %bitcast_add_fusion.2 = f32[384,4,2,128]{0,3,2,1:T(8,128)S(1)} fusion(f32[384,4,2,128]{0,3,2,1:T(8,128)S(1)} %get-tuple-element.276, bf16[1024,4,128,1]{0,2,3,1:T(8,128)(2,1)S(1)} %bitcast.149, f32[4,2,1024,384]{3,2,1,0:T(8,128)S(1)} %copy-done, f32[384,4,2]{0,2,1:T(2,128)S(1)} %fusion.87, pred[384,1024]{0,1:T(8,128)(4,1)S(1)} %broadcast_compare_fusion.2, ...), kind=kOutput, calls=%fused_computation.11.clone.1 | convolution fusion | flops 822214656 | bytes 17195008 | tf_op jit(solution)/shard_map/while/body/eval_jaxpr/ihcj,jhe->ihce/dot_general | solution.py:56
  215.9 0.3 broadcast_compare_fusion.2
  216.2 1.7 constant_dynamic-slice_fusion.3
  217.9 6.7 %fusion.86 = (f32[384,4,2]{0,2,1:T(2,128)S(1)}, f32[4,2,1024,384]{3,2,1,0:T(8,128)}) fusion(pred[384,1024]{0,1:T(8,128)(4,1)S(1)} %broadcast_compare_fusion.2, bf16[1024,4,2,64]{0,3,2,1:T(8,128)(2,1)S(1)} %bitcast.148, bf16[384,4,2,64]{0,3,2,1:T(8,128)(2,1)S(1)} %get-tuple-element.290), kind=kOutput, calls=%fused_computation.6.clone.1 | convolution fusion | flops 412087296 | bytes 14430208 | tf_op jit(solution)/shard_map/while/body/eval_jaxpr/ihcd,jhcd->ihcj/dot_general | solution.py:44
  224.6 6.8 %fusion.88 = f32[384,4,2]{0,2,1:T(2,128)S(1)} fusion(f32[4,2,1024,384]{3,2,1,0:T(8,128)} %get-tuple-element.257, f32[384,4,2]{0,2,1:T(2,128)S(1)} %fusion.87, pred[384,1024]{0,1:T(8,128)(4,1)S(1)} %broadcast_compare_fusion.2), kind=kLoop, calls=%fused_computation.8.clone.1 | loop fusion | flops 15725568 | bytes 13000704 | tf_op jit(solution)/shard_map/while/body/eval_jaxpr/reduce_sum | solution.py:55
  231.4 1.4 copy-done
  232.8 3.6 %bitcast_add_fusion.2 = f32[384,4,2,128]{0,3,2,1:T(8,128)S(1)} fusion(f32[384,4,2,128]{0,3,2,1:T(8,128)S(1)} %get-tuple-element.276, bf16[1024,4,128,1]{0,2,3,1:T(8,128)(2,1)S(1)} %bitcast.149, f32[4,2,1024,384]{3,2,1,0:T(8,128)S(1)} %copy-done, f32[384,4,2]{0,2,1:T(2,128)S(1)} %fusion.87, pred[384,1024]{0,1:T(8,128)(4,1)S(1)} %broadcast_compare_fusion.2, ...), kind=kOutput, calls=%fused_computation.11.clone.1 | convolution fusion | flops 822214656 | bytes 17195008 | tf_op jit(solution)/shard_map/while/body/eval_jaxpr/ihcj,jhe->ihce/dot_general | solution.py:56
  236.4 0.1 broadcast_divide_fusion
  236.5 0.2 fusion.64
  236.8 0.1 fusion.69
  236.9 0.1 mul.183
  236.9 1.0 multiply_convert_fusion
  238.0 0.0 all-gather.14.cloned.1.call-done
  238.0 6.1 %fusion.38 = bf16[8,1,64,1024]{3,2,1,0:T(8,128)(2,1)} fusion(bf16[1,2048,1024]{2,1,0:T(8,128)(2,1)} %param.27, bf16[8,1,64,2048]{3,2,0,1:T(8,128)(2,1)} %all-gather.14.cloned.1.call-done), kind=kOutput, calls=%fused_computation.43 | convolution fusion | flops 2148007936 | bytes 7340032 | tf_op jit(solution)/shard_map/sxcf,xfd->sxcd/dot_general | solution.py:124
  244.1 5.3 %all-to-all-start.1 = ((bf16[8,1,64,1024]{3,2,1,0:T(8,128)(2,1)}), bf16[8,1,64,1024]{3,2,1,0:T(8,128)(2,1)S(1)}, u32[]{:S(2)}, u32[]{:S(2)}) async-start(bf16[8,1,64,1024]{3,2,1,0:T(8,128)(2,1)} %fusion.38), calls=%async_computation.1 | async-start | bytes 2097152 | tf_op jit(solution)/shard_map/all_to_all | solution.py:131
  249.4 0.1 copy.40
  249.5 20.4 %all-gather.10.cloned.1.call-done = bf16[1,1,384,2048]{2,3,1,0:T(8,128)(2,1)} async-done(((bf16[1,1,384,512]{2,3,1,0:T(8,128)(2,1)}), bf16[1,1,384,2048]{2,3,1,0:T(8,128)(2,1)}) %all-gather.10.cloned.1.call-update) | async-done | bytes 1572880 | tf_op jit(solution)/shard_map/all_gather | solution.py:117
  269.9 5.4 %fusion.35 = bf16[384,1024]{1,0:T(8,128)(2,1)} fusion(bf16[2048,1024]{1,0:T(8,128)(2,1)} %param.20, bf16[1,1,384,2048]{2,3,1,0:T(8,128)(2,1)} %all-gather.10.cloned.1.call-done), kind=kOutput, calls=%fused_computation.42 | convolution fusion | flops 1611005952 | bytes 6553600 | tf_op jit(solution)/shard_map/dot_general | solution.py:116
  275.2 1.2 gather_fusion.1
  276.4 0.7 reshape.247
  277.1 2.1 multiply_reduce_fusion
  (50 shorter events, 0.4 us)
Async XLA Ops:
  7.2 90.4 %all-gather.12.cloned.1.call-start = ((), (), s32[]{:S(2)}) async-start(), calls=%async_computation.5 | async-start | bytes 5242880 | tf_op jit(solution)/shard_map/all_gather | solution.py:109
  12.6 31.4 %copy-start.2 = (bf16[384,512]{1,0:T(8,128)(2,1)S(1)}, bf16[384,512]{1,0:T(8,128)(2,1)}, u32[]{:S(2)}) copy-start(bf16[384,512]{1,0:T(8,128)(2,1)} %param.16) | copy-start | bytes 1179652
  14.7 30.3 %copy-start.3 = (bf16[384,512]{1,0:T(8,128)(2,1)S(1)}, bf16[384,512]{1,0:T(8,128)(2,1)}, u32[]{:S(2)}) copy-start(bf16[384,512]{1,0:T(8,128)(2,1)} %param.17) | copy-start | bytes 1179652
  14.7 32.5 %copy-start.4 = (f32[4]{0:T(128)S(1)}, f32[4]{0:T(128)}, u32[]{:S(2)}) copy-start(f32[4]{0:T(128)} %param.18) | copy-start | bytes 52
  14.7 32.5 %copy-start.6 = (f32[128]{0:T(128)S(1)}, f32[128]{0:T(128)}, u32[]{:S(2)}) copy-start(f32[128]{0:T(128)} %param.19) | copy-start | bytes 1540
  43.9 57.0 %copy-start.8 = (f32[4096]{0:T(1024)S(1)}, f32[4096]{0:T(1024)}, u32[]{:S(2)}) copy-start(f32[4096]{0:T(1024)} %param.22) | copy-start | bytes 49156
  43.9 91.5 %all-gather.6.cloned.1.call-start = ((), (), s32[]{:S(2)}) async-start(), calls=%async_computation.2 | async-start | bytes 3538944 | tf_op jit(solution)/shard_map/all_gather | solution.py:69
  44.9 129.2 %all-gather.8.cloned.1.call-start = ((), (), s32[]{:S(2)}) async-start(), calls=%async_computation.3 | async-start | bytes 3538944 | tf_op jit(solution)/shard_map/all_gather | solution.py:70
  45.9 192.1 %all-gather.14.cloned.1.call-start = ((), (), s32[]{:S(2)}) async-start(), calls=%async_computation.6 | async-start | bytes 2621440 | tf_op jit(solution)/shard_map/all_gather | solution.py:126
  97.6 3.4 %copy-start.1 = (bf16[8,1,64,4096]{3,2,1,0:T(8,128)(2,1)S(1)}, bf16[8,1,64,4096]{3,2,1,0:T(8,128)(2,1)}, u32[]{:S(2)}) copy-start(bf16[8,1,64,4096]{3,2,1,0:T(8,128)(2,1)} %all-gather.12.cloned.1.call-done) | copy-start | bytes 12582916
  101.1 4.7 %copy-start.7 = (bf16[1,4096,512]{2,1,0:T(8,128)(2,1)S(1)}, bf16[1,4096,512]{2,1,0:T(8,128)(2,1)}, u32[]{:S(2)}) copy-start(bf16[1,4096,512]{2,1,0:T(8,128)(2,1)} %param.26) | copy-start | bytes 12582916
  109.1 160.8 %all-gather.10.cloned.1.call-start = ((), (), s32[]{:S(2)}) async-start(), calls=%async_computation.4 | async-start | bytes 1966080 | tf_op jit(solution)/shard_map/all_gather | solution.py:117
  182.8 8.8 %copy-start = (f32[4,2,1024,384]{3,2,1,0:T(8,128)S(1)}, f32[4,2,1024,384]{3,2,1,0:T(8,128)}, u32[]{:S(2)}) copy-start(f32[4,2,1024,384]{3,2,1,0:T(8,128)} %get-tuple-element.257) | copy-start | bytes 37748740 | tf_op jit(solution)/shard_map/while
  204.0 8.3 %copy-start = (f32[4,2,1024,384]{3,2,1,0:T(8,128)S(1)}, f32[4,2,1024,384]{3,2,1,0:T(8,128)}, u32[]{:S(2)}) copy-start(f32[4,2,1024,384]{3,2,1,0:T(8,128)} %get-tuple-element.257) | copy-start | bytes 37748740 | tf_op jit(solution)/shard_map/while
  224.6 8.3 %copy-start = (f32[4,2,1024,384]{3,2,1,0:T(8,128)S(1)}, f32[4,2,1024,384]{3,2,1,0:T(8,128)}, u32[]{:S(2)}) copy-start(f32[4,2,1024,384]{3,2,1,0:T(8,128)} %get-tuple-element.257) | copy-start | bytes 37748740 | tf_op jit(solution)/shard_map/while
  237.9 11.5 %copy-start.5 = (f32[128,2]{0,1:T(2,128)S(1)}, f32[128,2]{0,1:T(2,128)}, u32[]{:S(2)}) copy-start(f32[128,2]{0,1:T(2,128)} %param.24) | copy-start | bytes 3076
  244.1 31.1 %all-to-all-start.1 = ((bf16[8,1,64,1024]{3,2,1,0:T(8,128)(2,1)}), bf16[8,1,64,1024]{3,2,1,0:T(8,128)(2,1)S(1)}, u32[]{:S(2)}, u32[]{:S(2)}) async-start(bf16[8,1,64,1024]{3,2,1,0:T(8,128)(2,1)} %fusion.38), calls=%async_computation.1 | async-start | bytes 2097152 | tf_op jit(solution)/shard_map/all_to_all | solution.py:131
Sparse Core Ops, SparseCore 0:
  44.0 53.5 all-gather.11
  99.2 36.1 all-gather.5
  137.0 37.0 all-gather.7
  176.4 36.0 all-gather.13
  238.1 31.7 all-gather.9
where the time goes:
time: 288 us; the launch traced here: 286 us
  waiting for transfers between devices  136 us (47%)
  matrix products  50.1 us (17%)
  other arithmetic  29.7 us (10%)
  blocking collectives  29.2 us (10%)
  local copies, waits for them, and re-layouts  21.2 us (7%)
  between operations  14 us (5%)
  starting transfers between devices  5.68 us (2%)
    all_gather x1, waiting for transfers between devices, per_device(): lax.all_gather(column_parts, 'tp', axis=3, tiled=True)  50.3 us
    all_gather x1, waiting for transfers between devices, per_device(): value_part = lax.all_gather(value_rows, 'ep', axis=0, tiled=True)  38.8 us
    all_to_all x1, blocking collectives, per_device(): lax.all_to_all(outgoing, 'ep', split_axis=0, concat_axis=0, tiled=True)  29.2 us
    all_gather x1, waiting for transfers between devices, per_device(): key_part = lax.all_gather(key_rows, 'ep', axis=0, tiled=True)  26.1 us
    reduce_sum x3, other arithmetic, key_block(): new_sum = old_sum * shrink + jnp.sum(weights, axis=-1)  20.6 us
    all_gather x1, waiting for transfers between devices, per_device(): lax.all_gather(head_out.reshape(1, 1, count_a, head_out.shape[1]), 'tp',...  20.4 us
    dot_general x3, matrix products, key_block(): jnp.einsum('ihcd,jhcd->ihcj', query_four, key_four, preferred_element_typ...  20 us
    dot_general x3, matrix products, key_block(): jnp.einsum('ihcj,jhe->ihce', weights.astype(jnp.bfloat16), value_three, p...  10.7 us
  transfers between devices with their start and end apart: 6, of which 4 were waited for; matrix products, arithmetic and copies ran while one was open for 30% of the time, Pallas kernels for 0%

commit v1 on v0

v1 whole, which is shorter than its diff:
```python
import functools

import jax
import jax.numpy as jnp
from jax import lax
from jax.experimental import pallas as pl
from jax.experimental.pallas import tpu as pltpu
from jax.sharding import PartitionSpec as P

eps = 1e-06
head_factor = 0.8
neg_big = -1e30
lanes = 2
f32 = jnp.float32
bf16 = jnp.bfloat16


def dot(a, b):
    return jnp.dot(a, b, preferred_element_type=f32)


def layer_kernel(
    n_ep,
    n_tp,
    scale_ref,
    q_hbm,
    k_hbm,
    v_hbm,
    gain_ref,
    wo_hbm,
    rows_hbm,
    norm_ref,
    ids_row_hbm,
    ids_col_ref,
    route_w_ref,
    wg_hbm,
    wu_hbm,
    wd_hbm,
    mixer_ref,
    mix_ref,
    q_in,
    q_two,
    k_all,
    v_all,
    rows_all,
    ids_all,
    arr,
    normed,
    hid_all,
    out_e,
    ret,
    head_all,
    acc,
    run_max,
    run_sum,
    wg,
    wu,
    wd,
    wo,
    local_sem,
    weight_sem,
    rows_up,
    rows_down,
    rows_side,
    rows_recv,
    ids_send,
    ids_recv,
    kv_up,
    kv_side,
    kv_recv,
    arr_send,
    arr_recv,
    hid_send,
    hid_recv,
    head_send,
    head_recv,
    ret_send,
    ret_recv,
):
    e = lax.axis_index("ep")
    t = lax.axis_index("tp")
    n_z = n_ep // lanes
    z = lax.div(e, lanes)
    c = lax.rem(e, lanes)
    partner = z * lanes + (1 - c)
    n_tok = q_in.shape[0]
    tok_b = rows_all.shape[1]
    per_head = acc.shape[0]
    head_w = q_two.shape[2]
    val_w = acc.shape[2]
    cap = ret.shape[1]
    slots = n_ep * cap
    cols = arr.shape[2]
    hidden_w = hid_all.shape[2]
    route_count = ids_col_ref.shape[1]

    def remote(src, dst, send, recv, ep_to, tp_to):
        return pltpu.make_async_remote_copy(
            src_ref=src,
            dst_ref=dst,
            send_sem=send,
            recv_sem=recv,
            device_id=(ep_to, tp_to),
            device_id_type=pl.DeviceIdType.MESH,
        )

    loads = [
        pltpu.make_async_copy(rows_hbm, rows_all.at[e], local_sem.at[0]),
        pltpu.make_async_copy(ids_row_hbm, ids_all.at[e], local_sem.at[1]),
        pltpu.make_async_copy(k_hbm, k_all.at[e], local_sem.at[2]),
        pltpu.make_async_copy(v_hbm, v_all.at[e], local_sem.at[3]),
        pltpu.make_async_copy(q_hbm, q_in, local_sem.at[4]),
    ]
    for load in loads:
        load.start()
    weights = [
        pltpu.make_async_copy(wg_hbm.at[0], wg, weight_sem.at[0]),
        pltpu.make_async_copy(wu_hbm.at[0], wu, weight_sem.at[1]),
        pltpu.make_async_copy(wd_hbm.at[0], wd, weight_sem.at[2]),
        pltpu.make_async_copy(wo_hbm, wo, weight_sem.at[3]),
    ]

    barrier = pltpu.get_barrier_semaphore()

    def greet_ep(i, carry):
        to = lax.rem(e + i, n_ep)
        pl.semaphore_signal(barrier, inc=1, device_id=(to, t), device_id_type=pl.DeviceIdType.MESH)
        return carry

    def greet_tp(i, carry):
        to = lax.rem(t + i, n_tp)
        pl.semaphore_signal(barrier, inc=1, device_id=(e, to), device_id_type=pl.DeviceIdType.MESH)
        return carry

    lax.fori_loop(1, n_ep, greet_ep, 0)
    lax.fori_loop(1, n_tp, greet_tp, 0)
    pl.semaphore_wait(barrier, n_ep - 1 + n_tp - 1)
    for load in loads:
        load.wait()

    def ids_copy(to):
        return remote(ids_all.at[e], ids_all.at[e], ids_send.at[to], ids_recv.at[e], to, t)

    def ids_arrival(b):
        return remote(ids_all.at[b], ids_all.at[b], ids_send.at[b], ids_recv.at[b], b, t)

    def rows_copy(block, send, to):
        return remote(rows_all.at[block], rows_all.at[block], send, rows_recv.at[block], to, t)

    def rows_copy_up(j):
        return rows_copy(j * lanes + c, rows_up.at[j], lax.rem(e + lanes, n_ep))

    def rows_copy_down(j):
        return rows_copy(j * lanes + c, rows_down.at[j], lax.rem(e + n_ep - lanes, n_ep))

    def rows_copy_side(j):
        return rows_copy(j * lanes + c, rows_side.at[j], partner)

    def kv_copies(j, sems, to):
        block = j * lanes + c
        return [
            remote(ref.at[block], ref.at[block], sems.at[i, j], kv_recv.at[i, block], to, t)
            for i, ref in enumerate((k_all, v_all))
        ]

    def kv_copies_up(j):
        return kv_copies(j, kv_up, lax.rem(e + lanes, n_ep))

    def kv_copies_side(j):
        return kv_copies(j, kv_side, partner)

    def kv_wait(block):
        for i, ref in enumerate((k_all, v_all)):
            remote(
                ref.at[block], ref.at[block], kv_up.at[i, 0], kv_recv.at[i, block], partner, t
            ).wait_recv()

    def arr_piece(block):
        return arr.at[t, pl.ds(pl.multiple_of(block * cap, cap), cap)]

    def tp_copy(buf, send, recv, source, to):
        return remote(buf.at[source], buf.at[source], send.at[to], recv.at[source], e, to)

    def tp_send_all(buf, send, recv):
        def one(i, carry):
            tp_copy(buf, send, recv, t, lax.rem(t + i, n_tp)).start()
            return carry

        lax.fori_loop(1, n_tp, one, 0)

    def tp_wait_recv(buf, send, recv):
        def one(i, carry):
            other = lax.rem(t + i, n_tp)
            tp_copy(buf, send, recv, other, other).wait_recv()
            return carry

        lax.fori_loop(1, n_tp, one, 0)

    def tp_wait_send(buf, send, recv):
        def one(i, carry):
            tp_copy(buf, send, recv, t, lax.rem(t + i, n_tp)).wait_send()
            return carry

        lax.fori_loop(1, n_tp, one, 0)

    def ret_copy(to):
        return remote(
            out_e.at[pl.ds(pl.multiple_of(to * cap, cap), cap)],
            ret.at[e],
            ret_send.at[to],
            ret_recv.at[e],
            to,
            t,
        )

    def ret_arrival(b):
        return remote(ret.at[b], ret.at[b], ret_send.at[b], ret_recv.at[b], b, t)

    def each_ep(work):
        def one(i, carry):
            work(lax.rem(e + i, n_ep))
            return carry

        lax.fori_loop(1, n_ep, one, 0)

    each_ep(lambda to: ids_copy(to).start())

    def pick(block):
        ids = ids_all[block]
        hit = (ids[0:1] == e).astype(f32)
        for k in range(1, route_count):
            hit = hit + (ids[k : k + 1] == e).astype(f32)
        before = (
            lax.broadcasted_iota(jnp.int32, (tok_b, tok_b), 0)
            < lax.broadcasted_iota(jnp.int32, (tok_b, tok_b), 1)
        ).astype(bf16)
        ranks = dot(jnp.broadcast_to(hit, (16, tok_b)).astype(bf16), before)[0:1]
        slot = lax.broadcasted_iota(jnp.int32, (cap, tok_b), 0).astype(f32)
        chosen = jnp.where((slot == ranks) & (hit > 0.5), 1.0, 0.0).astype(bf16)
        start = pl.multiple_of(block * cap, cap)
        arr[t, pl.ds(start, cap)] = dot(chosen, rows_all[block]).astype(bf16)

        def one(i, carry):
            to = lax.rem(t + i, n_tp)
            remote(arr_piece(block), arr_piece(block), arr_send.at[to], arr_recv.at[t], e, to).start()
            return carry

        lax.fori_loop(1, n_tp, one, 0)

    def rows_step(s, carry):
        low, high = z - s, z + s

        @pl.when((s > 0) & (low >= 0))
        def _():
            rows_copy_down(low).wait_recv()

        @pl.when((low >= 0) & (z + 1 < n_z))
        def _():
            rows_copy_up(low).start()

        @pl.when((s > 0) & (high < n_z))
        def _():
            rows_copy_up(high).wait_recv()

        @pl.when((high < n_z) & (z > 0))
        def _():
            rows_copy_down(high).start()

        @pl.when((s == z) & (z + 1 < n_z))
        def _():
            for copy in kv_copies_up(z):
                copy.start()

        @pl.when((s == z) & (c == 0))
        def _():
            for copy in kv_copies_side(z):
                copy.start()

        @pl.when(low >= 0)
        def _():
            rows_copy_side(low).start()

        @pl.when((s > 0) & (high < n_z))
        def _():
            rows_copy_side(high).start()

        def take(j):
            mine, other = j * lanes + c, j * lanes + (1 - c)

            @pl.when(j != z)
            def _():
                ids_arrival(mine).wait_recv()

            pick(mine)
            ids_arrival(other).wait_recv()
            rows_copy(other, rows_side.at[j], partner).wait_recv()
            pick(other)

        @pl.when(low >= 0)
        def _():
            take(low)

        @pl.when((s > 0) & (high < n_z))
        def _():
            take(high)

        return carry

    lax.fori_loop(0, n_z, rows_step, 0)
    for weight in weights:
        weight.start()

    lane = lax.broadcasted_iota(jnp.int32, (n_tok, head_w), 1)

    def split_maps(h, carry):
        scaled = q_in[:, pl.ds(pl.multiple_of(h * head_w, head_w), head_w)].astype(f32) * (
            (head_w // 2) ** -0.5
        )
        q_two[h, pl.ds(0, n_tok)] = jnp.where(lane < head_w // 2, scaled, 0.0).astype(bf16)
        q_two[h, pl.ds(n_tok, n_tok)] = jnp.where(lane < head_w // 2, 0.0, scaled).astype(bf16)
        return carry

    lax.fori_loop(0, per_head, split_maps, 0)

    def attend(block, own):
        def one(h, carry):
            keys = k_all[block, :, pl.ds(pl.multiple_of(h * head_w, head_w), head_w)]
            values = v_all[block, :, pl.ds(pl.multiple_of(h * val_w, val_w), val_w)]
            for m in range(2):
                part = pl.ds(m * n_tok, n_tok)
                scores = lax.dot_general(
                    q_two[h, part], keys, (((1,), (1,)), ((), ())), preferred_element_type=f32
                )
                if own:
                    scores = jnp.where(
                        lax.broadcasted_iota(jnp.int32, (n_tok, n_tok), 0)
                        >= lax.broadcasted_iota(jnp.int32, (n_tok, n_tok), 1),
                        scores,
                        neg_big,
                    )
                top = jnp.max(scores, axis=-1, keepdims=True)
                if not own:
                    old = run_max[h, part]
                    top = jnp.maximum(old, top)
                shares = jnp.exp(scores - top)
                total = jnp.sum(shares, axis=-1, keepdims=True)
                update = dot(shares.astype(bf16), values)
                if not own:
                    shrink = jnp.exp(old - top)
                    total = total + run_sum[h, part] * shrink
                    update = update + acc[h, part] * shrink
                run_max[h, part] = top
                run_sum[h, part] = total
                acc[h, part] = update
            return carry

        lax.fori_loop(0, per_head, one, 0)

    attend(e, True)

    @pl.when(c == 1)
    def _():
        kv_wait(partner)
        attend(partner, False)

    def kv_step(s, carry):
        j = z - s

        @pl.when(j >= 0)
        def _():
            kv_wait(j * lanes + c)

            @pl.when(z + 1 < n_z)
            def _():
                for copy in kv_copies_up(j):
                    copy.start()

            for copy in kv_copies_side(j):
                copy.start()
            attend(j * lanes + c, False)
            kv_wait(j * lanes + (1 - c))
            attend(j * lanes + (1 - c), False)

        return carry

    lax.fori_loop(1, n_z - 1, kv_step, 0)

    def arr_wait(i, carry):
        other = lax.rem(t + i, n_tp)
        tp_copy(arr, arr_send, arr_recv, other, other).wait_recv()
        return carry

    lax.fori_loop(1, n_tp, arr_wait, 0)
    for weight in weights:
        weight.wait()
    n_rows = min(slots, 64)

    def norm_step(i, carry):
        part = pl.ds(pl.multiple_of(i * n_rows, n_rows), n_rows)
        squares = jnp.zeros((n_rows, 1), f32)
        for p in range(n_tp):
            x = arr[p, part].astype(f32)
            squares = squares + jnp.sum(x * x, axis=-1, keepdims=True)
        factor = lax.rsqrt(squares / (n_tp * cols) + eps)
        for p in range(n_tp):
            where = pl.ds(p * cols, cols)
            normed[part, where] = (
                arr[p, part].astype(f32) * factor * norm_ref[0:1, where]
            ).astype(bf16)
        return carry

    lax.fori_loop(0, slots // n_rows, norm_step, 0)
    tile_f = min(hidden_w, 256)

    def gate_step(i, carry):
        where = pl.ds(pl.multiple_of(i * tile_f, tile_f), tile_f)
        gate = dot(normed[...], wg[:, where])
        up = dot(normed[...], wu[:, where])
        hid_all[t, :, where] = (gate / (1.0 + jnp.exp(-gate)) * up).astype(bf16)
        return carry

    lax.fori_loop(0, hidden_w // tile_f, gate_step, 0)
    tp_send_all(hid_all, hid_send, hid_recv)

    lax.fori_loop(n_z - 1, n_z, kv_step, 0)

    def head_step(h, carry):
        first = acc[h, pl.ds(0, n_tok)] / run_sum[h, pl.ds(0, n_tok)]
        second = acc[h, pl.ds(n_tok, n_tok)] / run_sum[h, pl.ds(n_tok, n_tok)]
        mixed = first - scale_ref[h] * second
        mean_sq = jnp.mean(mixed * mixed, axis=-1, keepdims=True)
        head_all[t, :, pl.ds(pl.multiple_of(h * val_w, val_w), val_w)] = (
            mixed * lax.rsqrt(mean_sq + eps) * gain_ref[0:1] * head_factor
        ).astype(bf16)
        return carry

    lax.fori_loop(0, per_head, head_step, 0)
    tp_send_all(head_all, head_send, head_recv)

    tp_wait_recv(hid_all, hid_send, hid_recv)
    out_w = out_e.shape[1]
    tile_o = min(out_w, 256)

    def down_step(i, carry):
        where = pl.ds(pl.multiple_of(i * tile_o, tile_o), tile_o)
        total = dot(hid_all[0], wd[pl.ds(0, hidden_w), where])
        for p in range(1, n_tp):
            total = total + dot(hid_all[p], wd[pl.ds(p * hidden_w, hidden_w), where])
        out_e[:, where] = total.astype(bf16)
        return carry

    lax.fori_loop(0, out_w // tile_o, down_step, 0)
    each_ep(lambda to: ret_copy(to).start())
    ret[e] = out_e[pl.ds(pl.multiple_of(e * cap, cap), cap)]

    tp_wait_recv(head_all, head_send, head_recv)
    heads_w = head_all.shape[2]

    def mixer_step(i, carry):
        where = pl.ds(pl.multiple_of(i * tile_o, tile_o), tile_o)
        total = dot(head_all[0], wo[pl.ds(0, heads_w), where])
        for p in range(1, n_tp):
            total = total + dot(head_all[p], wo[pl.ds(p * heads_w, heads_w), where])
        mixer_ref[:, where] = total.astype(bf16)
        return carry

    lax.fori_loop(0, out_w // tile_o, mixer_step, 0)

    each_ep(lambda b: ret_arrival(b).wait_recv())
    after = (
        lax.broadcasted_iota(jnp.int32, (tok_b, tok_b), 0)
        > lax.broadcasted_iota(jnp.int32, (tok_b, tok_b), 1)
    ).astype(bf16)

    def mix_step(b, total):
        hit = jnp.zeros((tok_b, 1), f32)
        share = jnp.zeros((tok_b, 1), f32)
        for k in range(route_count):
            named = ids_col_ref[:, k : k + 1] == b
            hit = hit + named.astype(f32)
            share = share + jnp.where(named, route_w_ref[:, k : k + 1], 0.0)
        ranks = dot(after, jnp.broadcast_to(hit, (tok_b, tok_b)).astype(bf16))[:, :cap]
        slot = lax.broadcasted_iota(jnp.int32, (tok_b, cap), 1).astype(f32)
        chosen = jnp.where((slot == ranks) & (hit > 0.5), 1.0, 0.0).astype(bf16)
        return total + share * dot(chosen, ret[b])

    mix_ref[...] = lax.fori_loop(0, n_ep, mix_step, jnp.zeros((tok_b, out_w), f32)).astype(bf16)

    each_ep(lambda to: ids_copy(to).wait_send())
    each_ep(lambda to: ret_copy(to).wait_send())
    tp_wait_send(arr, arr_send, arr_recv)
    tp_wait_send(hid_all, hid_send, hid_recv)
    tp_wait_send(head_all, head_send, head_recv)

    def drain(j, carry):
        rows_copy_side(j).wait_send()

        @pl.when((j <= z) & (z + 1 < n_z))
        def _():
            rows_copy_up(j).wait_send()
            for copy in kv_copies_up(j):
                copy.wait_send()

        @pl.when((j >= z) & (z > 0))
        def _():
            rows_copy_down(j).wait_send()

        @pl.when((j < z) | ((j == z) & (c == 0)))
        def _():
            for copy in kv_copies_side(j):
                copy.wait_send()

        return carry

    lax.fori_loop(0, n_z, drain, 0)


def per_device(
    n_ep,
    n_tp,
    query_rows,
    key_rows,
    value_rows,
    second_scale,
    head_gain,
    out_weight,
    routed_rows,
    norm_gain,
    route_ids,
    route_weight,
    expert_gate,
    expert_up,
    expert_down,
):
    n_tok, attn_w = query_rows.shape
    per_head = second_scale.shape[0]
    val_w = head_gain.shape[0]
    head_w = attn_w // per_head
    tok_b, cols = routed_rows.shape
    route_count = route_ids.shape[1]
    hidden_w = expert_gate.shape[2]
    out_w = out_weight.shape[1]
    n_z = n_ep // lanes
    cap = 2 * tok_b * route_count // n_ep
    slots = n_ep * cap
    ids_row = jnp.pad(route_ids.T, ((0, 8 - route_count), (0, 0)))
    vmem = pl.BlockSpec(memory_space=pltpu.VMEM)
    hbm = pl.BlockSpec(memory_space=pl.ANY)
    dma = pltpu.SemaphoreType.DMA
    return pl.pallas_call(
        functools.partial(layer_kernel, n_ep, n_tp),
        out_shape=(
            jax.ShapeDtypeStruct((n_tok, out_w), bf16),
            jax.ShapeDtypeStruct((tok_b, out_w), bf16),
        ),
        in_specs=[
            pl.BlockSpec(memory_space=pltpu.SMEM),
            hbm,
            hbm,
            hbm,
            vmem,
            hbm,
            hbm,
            vmem,
            hbm,
            vmem,
            vmem,
            hbm,
            hbm,
            hbm,
        ],
        out_specs=(vmem, vmem),
        scratch_shapes=[
            pltpu.VMEM((n_tok, attn_w), bf16),
            pltpu.VMEM((per_head, 2 * n_tok, head_w), bf16),
            pltpu.VMEM((n_ep, n_tok, attn_w), bf16),
            pltpu.VMEM((n_ep, n_tok, value_rows.shape[1]), bf16),
            pltpu.VMEM((n_ep, tok_b, cols), bf16),
            pltpu.VMEM((n_ep, 8, tok_b), jnp.int32),
            pltpu.VMEM((n_tp, slots, cols), bf16),
            pltpu.VMEM((slots, n_tp * cols), bf16),
            pltpu.VMEM((n_tp, slots, hidden_w), bf16),
            pltpu.VMEM((slots, out_w), bf16),
            pltpu.VMEM((n_ep, cap, out_w), bf16),
            pltpu.VMEM((n_tp, n_tok, per_head * val_w), bf16),
            pltpu.VMEM((per_head, 2 * n_tok, val_w), f32),
            pltpu.VMEM((per_head, 2 * n_tok, 1), f32),
            pltpu.VMEM((per_head, 2 * n_tok, 1), f32),
            pltpu.VMEM(expert_gate.shape[1:], bf16),
            pltpu.VMEM(expert_up.shape[1:], bf16),
            pltpu.VMEM(expert_down.shape[1:], bf16),
            pltpu.VMEM(out_weight.shape, bf16),
            dma((5,)),
            dma((4,)),
            dma((n_z,)),
            dma((n_z,)),
            dma((n_z,)),
            dma((n_ep,)),
            dma((n_ep,)),
            dma((n_ep,)),
            dma((2, n_z)),
            dma((2, n_z)),
            dma((2, n_ep)),
            dma((n_tp,)),
            dma((n_tp,)),
            dma((n_tp,)),
            dma((n_tp,)),
            dma((n_tp,)),
            dma((n_tp,)),
            dma((n_ep,)),
            dma((n_ep,)),
        ],
        compiler_params=pltpu.CompilerParams(
            collective_id=0, has_side_effects=True, vmem_limit_bytes=66000000
        ),
    )(
        second_scale,
        query_rows,
        key_rows,
        value_rows,
        head_gain.reshape(1, -1),
        out_weight,
        routed_rows,
        norm_gain.reshape(1, -1),
        ids_row,
        route_ids,
        route_weight,
        expert_gate,
        expert_up,
        expert_down,
    )


def solution(mesh):
    placed = (
        P("ep", "tp"),
        P("ep", "tp"),
        P("ep", "tp"),
        P("tp"),
        P(),
        P(None, "tp"),
        P("ep", "tp"),
        P(),
        P("ep", None),
        P("ep", None),
        P("ep", None, "tp"),
        P("ep", None, "tp"),
        P("ep", None, "tp"),
    )
    return jax.shard_map(
        functools.partial(per_device, mesh.shape["ep"], mesh.shape["tp"]),
        mesh=mesh,
        in_specs=placed,
        out_specs=(P("ep", "tp"), P("ep", "tp")),
        check_vma=False,
    )
```

time: 288 us -> 141 us (0.49)
  the two profiles are of different devices: /device:TPU:24 before, /device:TPU:17 now
where the time goes in v1:
time: 141 us; the launch traced here: 140 us
  Pallas kernels  132 us (94%)
  local copies, waits for them, and re-layouts  7.83 us (6%)
    pallas_call x1, Pallas kernels, per_device(): pl.pallas_call(functools.partial(layer_kernel, n_ep, n_tp), out_shape=(ja...  132 us
    unnamed x4, local copies, waits for them, and re-layouts  6.56 us

profile of v1, /device:TPU:17, one launch (start us, length us, event | category | flops | bytes accessed | tf_op | source)
XLA Modules:
  0.0 140.4 jit_solution(4061627274551018653)
XLA Ops:
  0.6 1.3 pad.4.ids_row_hbm
  1.9 1.4 %copy.16.route_w_ref = f32[128,2]{1,0:T(8,128)} copy(f32[128,2]{0,1:T(2,128)} %param.22) | data formatting | bytes 2048 | tf_op args[9]
  3.3 1.4 %copy.15.ids_col_ref = s32[128,2]{1,0:T(8,128)} copy(s32[128,2]{0,1:T(2,128)} %param.21) | data formatting | bytes 2048 | tf_op args[8]
  4.7 132.0 %shard_map.140 = (bf16[384,1024]{1,0:T(8,128)(2,1)}, bf16[128,1024]{1,0:T(8,128)(2,1)}) custom-call(f32[4]{0:T(128)} %scale_ref.1, bf16[384,512]{1,0:T(8,128)(2,1)} %q_hbm.1, bf16[384,512]{1,0:T(8,128)(2,1)} %k_hbm.1, bf16[384,512]{1,0:T(8,128)(2,1)} %v_hbm.1, f32[1,128]{1,0:T(1,128)} %bitcast.5, bf16[2048,1024]{1,0:T(8,128)(2,1)} %wo_hbm.1, ...), custom_call_target="tpu_custom_call" | custom-call | tf_op jit(solution)/shard_map/pallas_call | solution.py:550
  136.7 2.1 %copy.19 = bf16[384,1024]{1,0:T(8,128)(2,1)} copy(bf16[384,1024]{1,0:T(8,128)(2,1)} %get-tuple-element.4) | data formatting | bytes 1572864
  138.8 1.7 %copy.20 = bf16[128,1024]{1,0:T(8,128)(2,1)} copy(bf16[128,1024]{1,0:T(8,128)(2,1)} %get-tuple-element.5) | data formatting | bytes 524288

commit v2 on v1

--- a/solution.py
+++ b/solution.py
@@ -30,8 +30,7 @@
     wo_hbm,
     rows_hbm,
     norm_ref,
-    ids_row_hbm,
-    ids_col_ref,
+    ids_ref,
     route_w_ref,
     wg_hbm,
     wu_hbm,
@@ -50,6 +49,7 @@
     out_e,
     ret,
     head_all,
+    spread,
     acc,
     run_max,
     run_sum,
@@ -88,11 +88,12 @@
     per_head = acc.shape[0]
     head_w = q_two.shape[2]
     val_w = acc.shape[2]
-    cap = ret.shape[1]
-    slots = n_ep * cap
+    slots, out_w = ret.shape
+    cap = slots // n_ep
+    half = n_z // 2
     cols = arr.shape[2]
     hidden_w = hid_all.shape[2]
-    route_count = ids_col_ref.shape[1]
+    route_count = ids_ref.shape[0]
 
     def remote(src, dst, send, recv, ep_to, tp_to):
         return pltpu.make_async_remote_copy(
@@ -106,13 +107,13 @@
 
     loads = [
         pltpu.make_async_copy(rows_hbm, rows_all.at[e], local_sem.at[0]),
-        pltpu.make_async_copy(ids_row_hbm, ids_all.at[e], local_sem.at[1]),
-        pltpu.make_async_copy(k_hbm, k_all.at[e], local_sem.at[2]),
-        pltpu.make_async_copy(v_hbm, v_all.at[e], local_sem.at[3]),
-        pltpu.make_async_copy(q_hbm, q_in, local_sem.at[4]),
+        pltpu.make_async_copy(k_hbm, k_all.at[e], local_sem.at[1]),
+        pltpu.make_async_copy(v_hbm, v_all.at[e], local_sem.at[2]),
+        pltpu.make_async_copy(q_hbm, q_in, local_sem.at[3]),
     ]
     for load in loads:
         load.start()
+    ids_all[e, pl.ds(0, route_count)] = ids_ref[...]
     weights = [
         pltpu.make_async_copy(wg_hbm.at[0], wg, weight_sem.at[0]),
         pltpu.make_async_copy(wu_hbm.at[0], wu, weight_sem.at[1]),
@@ -175,46 +176,101 @@
                 ref.at[block], ref.at[block], kv_up.at[i, 0], kv_recv.at[i, block], partner, t
             ).wait_recv()
 
-    def arr_piece(block):
-        return arr.at[t, pl.ds(pl.multiple_of(block * cap, cap), cap)]
-
-    def tp_copy(buf, send, recv, source, to):
-        return remote(buf.at[source], buf.at[source], send.at[to], recv.at[source], e, to)
-
-    def tp_send_all(buf, send, recv):
+    square = n_tp == 4
+    across = t + 1 - 2 * lax.rem(t, 2)
+    along = lax.rem(t + 2, n_tp)
+    corner = n_tp - 1 - t
+
+    def piece(buf, source, i, units):
+        step = buf.shape[1] // (2 * units)
+        return buf.at[source, pl.ds(i * step, step)]
+
+    def tp_copy(buf, sems, units, source, i, row, to):
+        ref = piece(buf, source, i, units)
+        return remote(ref, ref, sems[0].at[row, i], sems[1].at[source, i], e, to)
+
+    def tp_peers(work):
         def one(i, carry):
-            tp_copy(buf, send, recv, t, lax.rem(t + i, n_tp)).start()
+            to = lax.rem(t + i, n_tp)
+            work(to, to)
             return carry
 
-        lax.fori_loop(1, n_tp, one, 0)
-
-    def tp_wait_recv(buf, send, recv):
-        def one(i, carry):
-            other = lax.rem(t + i, n_tp)
-            tp_copy(buf, send, recv, other, other).wait_recv()
-            return carry
-
-        lax.fori_loop(1, n_tp, one, 0)
-
-    def tp_wait_send(buf, send, recv):
-        def one(i, carry):
-            tp_copy(buf, send, recv, t, lax.rem(t + i, n_tp)).wait_send()
-            return carry
-
-        lax.fori_loop(1, n_tp, one, 0)
-
-    def ret_copy(to):
+        if square:
+            work(across, 0)
+            work(along, 1)
+        else:
+            lax.fori_loop(1, n_tp, one, 0)
+
+    def tp_send(buf, sems, units, unit):
+        for i in (2 * unit, 2 * unit + 1):
+            tp_peers(lambda to, row: tp_copy(buf, sems, units, t, i, row, to).start())
+
+    def tp_hand_on(buf, sems, units, unit):
+        if square:
+            i = 2 * unit
+            tp_copy(buf, sems, units, across, i, 2, across).wait_recv()
+            tp_copy(buf, sems, units, across, i, 2, along).start()
+            tp_copy(buf, sems, units, along, i + 1, 2, along).wait_recv()
+            tp_copy(buf, sems, units, along, i + 1, 2, across).start()
+
+    def tp_arrive(buf, sems, units, unit):
+        i = 2 * unit
+        if square:
+            for source, at in ((across, i + 1), (along, i), (corner, i), (corner, i + 1)):
+                tp_copy(buf, sems, units, source, at, 2, source).wait_recv()
+        else:
+            for at in (i, i + 1):
+                tp_peers(lambda to, row: tp_copy(buf, sems, units, to, at, row, to).wait_recv())
+
+    def tp_drain(buf, sems, units):
+        for i in range(2 * units):
+            tp_peers(lambda to, row: tp_copy(buf, sems, units, t, i, row, to).wait_send())
+            if square:
+                source, to = (across, along) if i % 2 == 0 else (along, across)
+                tp_copy(buf, sems, units, source, i, 2, to).wait_send()
+
+    arr_sems = (arr_send, arr_recv)
+    hid_sems = (hid_send, hid_recv)
+    head_sems = (head_send, head_recv)
+
+    def unit_of(j):
+        return lax.rem(lax.div(j, half) + lax.div(z, half), 2)
+
+    def first_slot(j, side):
+        return pl.multiple_of(((unit_of(j) * 2 + side) * half + lax.rem(j, half)) * cap, cap)
+
+    def ret_part(b):
+        return ret.at[pl.ds(pl.multiple_of(b * cap, cap), cap)]
+
+    def ret_copy(j, side):
+        to = j * lanes + (c if side == 0 else 1 - c)
         return remote(
-            out_e.at[pl.ds(pl.multiple_of(to * cap, cap), cap)],
-            ret.at[e],
+            out_e.at[pl.ds(first_slot(j, side), cap)],
+            ret_part(e),
             ret_send.at[to],
             ret_recv.at[e],
             to,
             t,
         )
 
+    def ret_each(unit, work):
+        def one(i, carry):
+            j = lax.rem(lax.div(z, half) + unit, 2) * half + i
+            if unit == 0:
+
+                @pl.when(j != z)
+                def _():
+                    work(ret_copy(j, 0))
+
+            else:
+                work(ret_copy(j, 0))
+            work(ret_copy(j, 1))
+            return carry
+
+        lax.fori_loop(0, half, one, 0)
+
     def ret_arrival(b):
-        return remote(ret.at[b], ret.at[b], ret_send.at[b], ret_recv.at[b], b, t)
+        return remote(ret_part(b), ret_part(b), ret_send.at[b], ret_recv.at[b], b, t)
 
     def each_ep(work):
         def one(i, carry):
@@ -225,7 +281,7 @@
 
     each_ep(lambda to: ids_copy(to).start())
 
-    def pick(block):
+    def pick(block, j, side):
         ids = ids_all[block]
         hit = (ids[0:1] == e).astype(f32)
         for k in range(1, route_count):
@@ -237,15 +293,15 @@
         ranks = dot(jnp.broadcast_to(hit, (16, tok_b)).astype(bf16), before)[0:1]
         slot = lax.broadcasted_iota(jnp.int32, (cap, tok_b), 0).astype(f32)
         chosen = jnp.where((slot == ranks) & (hit > 0.5), 1.0, 0.0).astype(bf16)
-        start = pl.multiple_of(block * cap, cap)
+        start = first_slot(j, side)
+        i = unit_of(j) * 2 + side
         arr[t, pl.ds(start, cap)] = dot(chosen, rows_all[block]).astype(bf16)
-
-        def one(i, carry):
-            to = lax.rem(t + i, n_tp)
-            remote(arr_piece(block), arr_piece(block), arr_send.at[to], arr_recv.at[t], e, to).start()
-            return carry
-
-        lax.fori_loop(1, n_tp, one, 0)
+        part = arr.at[t, pl.ds(start, cap)]
+        tp_peers(
+            lambda to, row: remote(
+                part, part, arr_send.at[row, i], arr_recv.at[t, i], e, to
+            ).start()
+        )
 
     def rows_step(s, carry):
         low, high = z - s, z + s
@@ -291,10 +347,10 @@
             def _():
                 ids_arrival(mine).wait_recv()
 
-            pick(mine)
+            pick(mine, j, 0)
             ids_arrival(other).wait_recv()
             rows_copy(other, rows_side.at[j], partner).wait_recv()
-            pick(other)
+            pick(other, j, 1)
 
         @pl.when(low >= 0)
         def _():
@@ -309,6 +365,7 @@
     lax.fori_loop(0, n_z, rows_step, 0)
     for weight in weights:
         weight.start()
+    tp_hand_on(arr, arr_sems, 2, 0)
 
     lane = lax.broadcasted_iota(jnp.int32, (n_tok, head_w), 1)
 
@@ -363,7 +420,9 @@
         kv_wait(partner)
         attend(partner, False)
 
-    def kv_step(s, carry):
+    tp_hand_on(arr, arr_sems, 2, 1)
+
+    def kv_pass(s, carry):
         j = z - s
 
         @pl.when(j >= 0)
@@ -377,52 +436,97 @@
 
             for copy in kv_copies_side(j):
                 copy.start()
+
+        return carry
+
+    def kv_attend(s, carry):
+        j = z - s
+
+        @pl.when(j >= 0)
+        def _():
             attend(j * lanes + c, False)
             kv_wait(j * lanes + (1 - c))
             attend(j * lanes + (1 - c), False)
 
         return carry
 
-    lax.fori_loop(1, n_z - 1, kv_step, 0)
-
-    def arr_wait(i, carry):
-        other = lax.rem(t + i, n_tp)
-        tp_copy(arr, arr_send, arr_recv, other, other).wait_recv()
-        return carry
-
-    lax.fori_loop(1, n_tp, arr_wait, 0)
+    lax.fori_loop(1, 2, kv_pass, 0)
+
     for weight in weights:
         weight.wait()
-    n_rows = min(slots, 64)
-
-    def norm_step(i, carry):
-        part = pl.ds(pl.multiple_of(i * n_rows, n_rows), n_rows)
-        squares = jnp.zeros((n_rows, 1), f32)
-        for p in range(n_tp):
-            x = arr[p, part].astype(f32)
-            squares = squares + jnp.sum(x * x, axis=-1, keepdims=True)
-        factor = lax.rsqrt(squares / (n_tp * cols) + eps)
-        for p in range(n_tp):
-            where = pl.ds(p * cols, cols)
-            normed[part, where] = (
-                arr[p, part].astype(f32) * factor * norm_ref[0:1, where]
-            ).astype(bf16)
-        return carry
-
-    lax.fori_loop(0, slots // n_rows, norm_step, 0)
+    unit_rows = slots // 2
+    n_rows = min(unit_rows, 64)
     tile_f = min(hidden_w, 256)
 
-    def gate_step(i, carry):
-        where = pl.ds(pl.multiple_of(i * tile_f, tile_f), tile_f)
-        gate = dot(normed[...], wg[:, where])
-        up = dot(normed[...], wu[:, where])
-        hid_all[t, :, where] = (gate / (1.0 + jnp.exp(-gate)) * up).astype(bf16)
-        return carry
-
-    lax.fori_loop(0, hidden_w // tile_f, gate_step, 0)
-    tp_send_all(hid_all, hid_send, hid_recv)
-
-    lax.fori_loop(n_z - 1, n_z, kv_step, 0)
+    def expert_in(unit):
+        tp_arrive(arr, arr_sems, 2, unit)
+
+        def norm_step(i, carry):
+            part = pl.ds(pl.multiple_of(unit * unit_rows + i * n_rows, n_rows), n_rows)
+            squares = jnp.zeros((n_rows, 1), f32)
+            for p in range(n_tp):
+                x = arr[p, part].astype(f32)
+                squares = squares + jnp.sum(x * x, axis=-1, keepdims=True)
+            factor = lax.rsqrt(squares / (n_tp * cols) + eps)
+            for p in range(n_tp):
+                where = pl.ds(p * cols, cols)
+                normed[part, where] = (
+                    arr[p, part].astype(f32) * factor * norm_ref[0:1, where]
+                ).astype(bf16)
+            return carry
+
+        lax.fori_loop(0, unit_rows // n_rows, norm_step, 0)
+        rows = pl.ds(unit * unit_rows, unit_rows)
+
+        def gate_step(i, carry):
+            where = pl.ds(pl.multiple_of(i * tile_f, tile_f), tile_f)
+            gate = dot(normed[rows], wg[:, where])
+            up = dot(normed[rows], wu[:, where])
+            hid_all[t, rows, where] = (gate / (1.0 + jnp.exp(-gate)) * up).astype(bf16)
+            return carry
+
+        lax.fori_loop(0, hidden_w // tile_f, gate_step, 0)
+        tp_send(hid_all, hid_sems, 2, unit)
+
+    expert_in(0)
+    expert_in(1)
+    lax.fori_loop(1, 2, kv_attend, 0)
+
+    @pl.when(z + 1 < n_z)
+    def _():
+        lax.fori_loop(2, n_z - 1, kv_pass, 0)
+
+    tp_hand_on(hid_all, hid_sems, 2, 0)
+    tp_hand_on(hid_all, hid_sems, 2, 1)
+    tile_o = min(out_w, 256)
+
+    def expert_out(unit):
+        tp_arrive(hid_all, hid_sems, 2, unit)
+        rows = pl.ds(unit * unit_rows, unit_rows)
+
+        def down_step(i, carry):
+            where = pl.ds(pl.multiple_of(i * tile_o, tile_o), tile_o)
+            total = dot(hid_all[0, rows], wd[pl.ds(0, hidden_w), where])
+            for p in range(1, n_tp):
+                total = total + dot(hid_all[p, rows], wd[pl.ds(p * hidden_w, hidden_w), where])
+            out_e[rows, where] = total.astype(bf16)
+            return carry
+
+        lax.fori_loop(0, out_w // tile_o, down_step, 0)
+        ret_each(unit, lambda copy: copy.start())
+
+    expert_out(0)
+    expert_out(1)
+    ret[pl.ds(pl.multiple_of(e * cap, cap), cap)] = out_e[pl.ds(first_slot(z, 0), cap)]
+
+    def kv_late(s, carry):
+        @pl.when(z + 1 == n_z)
+        def _():
+            kv_pass(s, 0)
+
+        return kv_attend(s, carry)
+
+    lax.fori_loop(2, n_z, kv_late, 0)
 
     def head_step(h, carry):
         first = acc[h, pl.ds(0, n_tok)] / run_sum[h, pl.ds(0, n_tok)]
@@ -435,25 +539,29 @@
         return carry
 
     lax.fori_loop(0, per_head, head_step, 0)
-    tp_send_all(head_all, head_send, head_recv)
-
-    tp_wait_recv(hid_all, hid_send, hid_recv)
-    out_w = out_e.shape[1]
-    tile_o = min(out_w, 256)
-
-    def down_step(i, carry):
-        where = pl.ds(pl.multiple_of(i * tile_o, tile_o), tile_o)
-        total = dot(hid_all[0], wd[pl.ds(0, hidden_w), where])
-        for p in range(1, n_tp):
-            total = total + dot(hid_all[p], wd[pl.ds(p * hidden_w, hidden_w), where])
-        out_e[:, where] = total.astype(bf16)
-        return carry
-
-    lax.fori_loop(0, out_w // tile_o, down_step, 0)
-    each_ep(lambda to: ret_copy(to).start())
-    ret[e] = out_e[pl.ds(pl.multiple_of(e * cap, cap), cap)]
-
-    tp_wait_recv(head_all, head_send, head_recv)
+    tp_send(head_all, head_sems, 1, 0)
+
+    row_of = lax.broadcasted_iota(jnp.int32, (tok_b, tok_b), 0)
+    col_of = lax.broadcasted_iota(jnp.int32, (tok_b, tok_b), 1)
+
+    def column(row):
+        return jnp.sum(
+            jnp.where(row_of == col_of, row.astype(f32), 0.0), axis=1, keepdims=True
+        )
+
+    shares = []
+    for k in range(route_count):
+        ids = column(ids_ref[k : k + 1])
+        same = jnp.zeros((tok_b, tok_b), f32)
+        for other in range(route_count):
+            same = same + (ids_ref[other : other + 1].astype(f32) == ids).astype(f32)
+        ranks = jnp.sum(jnp.where(col_of < row_of, same, 0.0), axis=1, keepdims=True)
+        slot = lax.broadcasted_iota(jnp.int32, (tok_b, slots), 1).astype(f32)
+        spread[k] = jnp.where(slot == ids * cap + ranks, 1.0, 0.0).astype(bf16)
+        shares.append(column(route_w_ref[k : k + 1]))
+
+    tp_hand_on(head_all, head_sems, 1, 0)
+    tp_arrive(head_all, head_sems, 1, 0)
     heads_w = head_all.shape[2]
 
     def mixer_step(i, carry):
@@ -467,30 +575,20 @@
     lax.fori_loop(0, out_w // tile_o, mixer_step, 0)
 
     each_ep(lambda b: ret_arrival(b).wait_recv())
-    after = (
-        lax.broadcasted_iota(jnp.int32, (tok_b, tok_b), 0)
-        > lax.broadcasted_iota(jnp.int32, (tok_b, tok_b), 1)
-    ).astype(bf16)
-
-    def mix_step(b, total):
-        hit = jnp.zeros((tok_b, 1), f32)
-        share = jnp.zeros((tok_b, 1), f32)
-        for k in range(route_count):
-            named = ids_col_ref[:, k : k + 1] == b
-            hit = hit + named.astype(f32)
-            share = share + jnp.where(named, route_w_ref[:, k : k + 1], 0.0)
-        ranks = dot(after, jnp.broadcast_to(hit, (tok_b, tok_b)).astype(bf16))[:, :cap]
-        slot = lax.broadcasted_iota(jnp.int32, (tok_b, cap), 1).astype(f32)
-        chosen = jnp.where((slot == ranks) & (hit > 0.5), 1.0, 0.0).astype(bf16)
-        return total + share * dot(chosen, ret[b])
-
-    mix_ref[...] = lax.fori_loop(0, n_ep, mix_step, jnp.zeros((tok_b, out_w), f32)).astype(bf16)
+    tile_m = min(out_w, 256)
+    for start in range(0, out_w, tile_m):
+        where = pl.ds(start, tile_m)
+        total = shares[0] * dot(spread[0], ret[:, where])
+        for k in range(1, route_count):
+            total = total + shares[k] * dot(spread[k], ret[:, where])
+        mix_ref[:, where] = total.astype(bf16)
 
     each_ep(lambda to: ids_copy(to).wait_send())
-    each_ep(lambda to: ret_copy(to).wait_send())
-    tp_wait_send(arr, arr_send, arr_recv)
-    tp_wait_send(hid_all, hid_send, hid_recv)
-    tp_wait_send(head_all, head_send, head_recv)
+    for unit in range(2):
+        ret_each(unit, lambda copy: copy.wait_send())
+    tp_drain(arr, arr_sems, 2)
+    tp_drain(hid_all, hid_sems, 2)
+    tp_drain(head_all, head_sems, 1)
 
     def drain(j, carry):
         rows_copy_side(j).wait_send()
@@ -543,7 +641,6 @@
     n_z = n_ep // lanes
     cap = 2 * tok_b * route_count // n_ep
     slots = n_ep * cap
-    ids_row = jnp.pad(route_ids.T, ((0, 8 - route_count), (0, 0)))
     vmem = pl.BlockSpec(memory_space=pltpu.VMEM)
     hbm = pl.BlockSpec(memory_space=pl.ANY)
     dma = pltpu.SemaphoreType.DMA
@@ -562,7 +659,6 @@
             hbm,
             hbm,
             vmem,
-            hbm,
             vmem,
             vmem,
             hbm,
@@ -581,8 +677,9 @@
             pltpu.VMEM((slots, n_tp * cols), bf16),
             pltpu.VMEM((n_tp, slots, hidden_w), bf16),
             pltpu.VMEM((slots, out_w), bf16),
-            pltpu.VMEM((n_ep, cap, out_w), bf16),
+            pltpu.VMEM((slots, out_w), bf16),
             pltpu.VMEM((n_tp, n_tok, per_head * val_w), bf16),
+            pltpu.VMEM((route_count, tok_b, slots), bf16),
             pltpu.VMEM((per_head, 2 * n_tok, val_w), f32),
             pltpu.VMEM((per_head, 2 * n_tok, 1), f32),
             pltpu.VMEM((per_head, 2 * n_tok, 1), f32),
@@ -590,7 +687,7 @@
             pltpu.VMEM(expert_up.shape[1:], bf16),
             pltpu.VMEM(expert_down.shape[1:], bf16),
             pltpu.VMEM(out_weight.shape, bf16),
-            dma((5,)),
+            dma((4,)),
             dma((4,)),
             dma((n_z,)),
             dma((n_z,)),
@@ -601,12 +698,12 @@
             dma((2, n_z)),
             dma((2, n_z)),
             dma((2, n_ep)),
-            dma((n_tp,)),
-            dma((n_tp,)),
-            dma((n_tp,)),
-            dma((n_tp,)),
-            dma((n_tp,)),
-            dma((n_tp,)),
+            dma((n_tp, 4)),
+            dma((n_tp, 4)),
+            dma((n_tp, 4)),
+            dma((n_tp, 4)),
+            dma((n_tp, 2)),
+            dma((n_tp, 2)),
             dma((n_ep,)),
             dma((n_ep,)),
         ],
@@ -622,9 +719,8 @@
         out_weight,
         routed_rows,
         norm_gain.reshape(1, -1),
-        ids_row,
-        route_ids,
-        route_weight,
+        route_ids.T,
+        route_weight.T,
         expert_gate,
         expert_up,
         expert_down,

time: 141 us -> 122 us (0.87)
  the two profiles are of different devices: /device:TPU:17 before, /device:TPU:24 now
where the time goes in v2:
time: 122 us
  Pallas kernels  118 us (97%)
  local copies, waits for them, and re-layouts  3.73 us (3%)
    pallas_call x1, Pallas kernels, per_device(): pl.pallas_call(functools.partial(layer_kernel, n_ep, n_tp), out_shape=(ja...  118 us
    unnamed x2, local copies, waits for them, and re-layouts  3.73 us

profile of v2, /device:TPU:24, one launch (start us, length us, event | category | flops | bytes accessed | tf_op | source)
XLA Modules:
  0.0 122.2 jit_solution(1850558242295395666)
XLA Ops:
  0.6 117.8 %shard_map.140 = (bf16[384,1024]{1,0:T(8,128)(2,1)}, bf16[128,1024]{1,0:T(8,128)(2,1)}) custom-call(f32[4]{0:T(128)} %scale_ref.1, bf16[384,512]{1,0:T(8,128)(2,1)} %q_hbm.1, bf16[384,512]{1,0:T(8,128)(2,1)} %k_hbm.1, bf16[384,512]{1,0:T(8,128)(2,1)} %v_hbm.1, f32[1,128]{1,0:T(1,128)} %bitcast.7, bf16[2048,1024]{1,0:T(8,128)(2,1)} %wo_hbm.1, ...), custom_call_target="tpu_custom_call" | custom-call | tf_op jit(solution)/shard_map/pallas_call | solution.py:647
  118.4 2.1 %copy.17 = bf16[384,1024]{1,0:T(8,128)(2,1)} copy(bf16[384,1024]{1,0:T(8,128)(2,1)} %get-tuple-element.4) | data formatting | bytes 1572864
  120.5 1.7 %copy.18 = bf16[128,1024]{1,0:T(8,128)(2,1)} copy(bf16[128,1024]{1,0:T(8,128)(2,1)} %get-tuple-element.5) | data formatting | bytes 524288

commit v3 on v2

--- a/solution.py
+++ b/solution.py
@@ -383,8 +383,12 @@
         def one(h, carry):
             keys = k_all[block, :, pl.ds(pl.multiple_of(h * head_w, head_w), head_w)]
             values = v_all[block, :, pl.ds(pl.multiple_of(h * val_w, val_w), val_w)]
-            for m in range(2):
-                part = pl.ds(m * n_tok, n_tok)
+            parts = [pl.ds(m * n_tok, n_tok) for m in range(2)]
+            held = []
+            if not own:
+                held = [(run_max[h, part], run_sum[h, part], acc[h, part]) for part in parts]
+            results = []
+            for m, part in enumerate(parts):
                 scores = lax.dot_general(
                     q_two[h, part], keys, (((1,), (1,)), ((), ())), preferred_element_type=f32
                 )
@@ -397,15 +401,17 @@
                     )
                 top = jnp.max(scores, axis=-1, keepdims=True)
                 if not own:
-                    old = run_max[h, part]
+                    old, old_sum, old_acc = held[m]
                     top = jnp.maximum(old, top)
                 shares = jnp.exp(scores - top)
                 total = jnp.sum(shares, axis=-1, keepdims=True)
                 update = dot(shares.astype(bf16), values)
                 if not own:
                     shrink = jnp.exp(old - top)
-                    total = total + run_sum[h, part] * shrink
-                    update = update + acc[h, part] * shrink
+                    total = total + old_sum * shrink
+                    update = update + old_acc * shrink
+                results.append((top, total, update))
+            for part, (top, total, update) in zip(parts, results):
                 run_max[h, part] = top
                 run_sum[h, part] = total
                 acc[h, part] = update
@@ -490,11 +496,11 @@
 
     expert_in(0)
     expert_in(1)
-    lax.fori_loop(1, 2, kv_attend, 0)
-
     @pl.when(z + 1 < n_z)
     def _():
         lax.fori_loop(2, n_z - 1, kv_pass, 0)
+
+    lax.fori_loop(1, 2, kv_attend, 0)
 
     tp_hand_on(hid_all, hid_sems, 2, 0)
     tp_hand_on(hid_all, hid_sems, 2, 1)

time: 122 us -> 122 us (level)
  no operation moved by 1% of the time
where the time goes in v3:
time: 122 us
  Pallas kernels  118 us (97%)
  local copies, waits for them, and re-layouts  3.73 us (3%)
    pallas_call x1, Pallas kernels, per_device(): pl.pallas_call(functools.partial(layer_kernel, n_ep, n_tp), out_shape=(ja...  118 us
    unnamed x2, local copies, waits for them, and re-layouts  3.73 us

profile of v3, /device:TPU:24, one launch (start us, length us, event | category | flops | bytes accessed | tf_op | source)
XLA Modules:
  0.0 122.2 jit_solution(11450791273176136189)
XLA Ops:
  0.6 117.8 %shard_map.140 = (bf16[384,1024]{1,0:T(8,128)(2,1)}, bf16[128,1024]{1,0:T(8,128)(2,1)}) custom-call(f32[4]{0:T(128)} %scale_ref.1, bf16[384,512]{1,0:T(8,128)(2,1)} %q_hbm.1, bf16[384,512]{1,0:T(8,128)(2,1)} %k_hbm.1, bf16[384,512]{1,0:T(8,128)(2,1)} %v_hbm.1, f32[1,128]{1,0:T(1,128)} %bitcast.7, bf16[2048,1024]{1,0:T(8,128)(2,1)} %wo_hbm.1, ...), custom_call_target="tpu_custom_call" | custom-call | tf_op jit(solution)/shard_map/pallas_call | solution.py:653
  118.4 2.1 %copy.17 = bf16[384,1024]{1,0:T(8,128)(2,1)} copy(bf16[384,1024]{1,0:T(8,128)(2,1)} %get-tuple-element.4) | data formatting | bytes 1572864
  120.5 1.7 %copy.18 = bf16[128,1024]{1,0:T(8,128)(2,1)} copy(bf16[128,1024]{1,0:T(8,128)(2,1)} %get-tuple-element.5) | data formatting | bytes 524288
